TPU v7x, 32 devices: a whole 2x2x4 slice. The times are simulated.
32 devices in a mesh: sp: 16 (over z, y, x), tp: 2 (over core).
Axes of the slice: x: 2, y: 2, z: 4, core: 2. Of those that a mesh axis runs over, the one named last changes fastest.
Arguments:
- resid: bfloat16 [2048, 2048], P(('sp', 'tp')), may hold values from -3 to 3
- queries: bfloat16 [2048, 2048], P('sp', 'tp'), may hold values from -6 to 6
- keys: bfloat16 [2048, 2048], P('sp', 'tp'), may hold values from -6 to 6
- values: bfloat16 [2048, 2048], P('sp', 'tp'), may hold values from -8 to 8
- doc_ids: int32 [2048], P('sp'), may hold values from 0 to 3, never falling along the last dimension, each value on 1 to 896 neighbouring positions
- score_offset: float32 [32], P('tp'), may hold values from -10 to -3
- out_weight: bfloat16 [2048, 2048], P('tp'), may hold values from -0.1875 to 0.1875
- norm_gain: float32 [2048], replicated, may hold values from 0.1 to 1.9
- gate_weight: bfloat16 [2048, 6144], P('sp', 'tp'), may hold values from -0.125 to 0.125
- up_weight: bfloat16 [2048, 6144], P('sp', 'tp'), may hold values from -0.125 to 0.125
- down_weight: bfloat16 [6144, 2048], P('tp', 'sp'), may hold values from -0.078125 to 0.078125
Outputs:
- layer_out: bfloat16 [2048, 2048], P(('sp', 'tp'))
Inputs may be any that keep to these rules, and one draw needn't show every extreme that they name: `doc_ids`: document numbers never fall along the sequence; each document has 1 to 896 positions, and one has exactly 896.
All inputs are finite; a program needn't handle non-finite values.
Results may differ from a plain program's by a relative error of at most 0.017.
Values may be sent and summed in bfloat16 or wider, within the bound.
A program may use at most 128 MiB of HBM per device.

v0:
```python
import jax
import jax.numpy as jnp
from jax import lax
from jax.sharding import PartitionSpec as P


def from_behind(shard, axis, by):
    peers = lax.axis_size(axis)
    pairs = [(i, i + by) for i in range(peers) if 0 <= i + by < peers]
    return lax.ppermute(shard, axis, pairs)


def as_sent(shard):
    return jax.tree.map(lambda a: a.astype(jnp.bfloat16) if a.dtype == jnp.float32 else a, shard)


def joined(earlier, later):
    return (
        jnp.concatenate([earlier[0], later[0]], axis=0),
        jnp.concatenate([earlier[1], later[1]], axis=0),
        jnp.concatenate([earlier[2], later[2]], axis=0),
    )


def block_update(carry, block, start, context):
    queries_h, q_pos, q_docs, offsets, scale = context
    total, carried = carry
    k_block, v_block, d_block = block
    count = k_block.shape[0]
    heads = offsets.shape[0]
    head_dim = queries_h.shape[2]

    def compute():
        key_pos = start + jnp.arange(count, dtype=jnp.int32)
        live = (
            (key_pos[None, :] >= 0)
            & (key_pos[None, :] < q_pos[:, None])
            & (d_block[None, :] == q_docs[:, None])
        )
        k_heads = k_block.reshape(count, heads, head_dim)
        v_heads = v_block.reshape(count, heads, head_dim)
        scores = (
            jnp.einsum("thd,shd->hts", queries_h, k_heads, preferred_element_type=jnp.float32)
            * scale
            + offsets[:, None, None]
        )
        log_keep = jnp.where(live[None], jax.nn.log_sigmoid(-scores), 0.0)
        tail = lax.cumsum(log_keep, axis=2, reverse=True) - log_keep + carried[:, :, None]
        weight = jnp.where(live[None], jnp.exp(jax.nn.log_sigmoid(scores) + tail), 0.0).astype(
            jnp.bfloat16
        )
        added = jnp.einsum("hts,shd->thd", weight, v_heads, preferred_element_type=jnp.float32)
        return (total + added, carried + jnp.sum(log_keep, axis=2))

    reached = (start + count > 0) & (d_block[-1] >= q_docs[0])
    return lax.cond(reached, compute, lambda: carry)


def on_device(
    resid,
    queries,
    keys,
    values,
    doc_ids,
    score_offset,
    out_weight,
    norm_gain,
    gate_weight,
    up_weight,
    down_weight,
):
    rows = queries.shape[0]
    heads = score_offset.shape[0]
    head_dim = queries.shape[1] // heads
    base = lax.axis_index("sp") * rows
    q_pos = base + jnp.arange(rows, dtype=jnp.int32)
    context = (
        queries.reshape(rows, heads, head_dim),
        q_pos,
        doc_ids,
        score_offset,
        head_dim ** (-0.5),
    )
    own = (keys, values, doc_ids)
    carry = (jnp.zeros((rows, heads, head_dim), jnp.float32), jnp.zeros((heads, rows), jnp.float32))
    nearest = from_behind((keys, values, doc_ids), "sp", 1)
    paired = joined(nearest, own)
    carry = block_update(carry, paired, base - rows, context)
    middle = from_behind((paired[0], paired[1], as_sent(paired[2])), "sp", 2)
    carry = block_update(carry, middle, base - 3 * rows, context)
    fourfold = joined(middle, paired)
    farthest = from_behind((fourfold[0], fourfold[1], as_sent(fourfold[2])), "sp", 4)
    carry = block_update(
        carry, tuple((piece[2 * rows :] for piece in farthest)), base - 5 * rows, context
    )
    carry = block_update(
        carry, tuple((piece[: 2 * rows] for piece in farthest)), base - 7 * rows, context
    )
    attended = carry[0].reshape(rows, heads * head_dim).astype(jnp.bfloat16)
    mixed_attn = lax.psum_scatter(
        jnp.dot(attended, out_weight, preferred_element_type=jnp.float32).astype(jnp.bfloat16),
        "tp",
        scatter_dimension=0,
        tiled=True,
    ).astype(jnp.float32)
    stream = resid.astype(jnp.float32) + mixed_attn
    normed = (
        stream * lax.rsqrt(jnp.mean(stream * stream, axis=1, keepdims=True) + 1e-06) * norm_gain
    ).astype(jnp.bfloat16)
    span_rows = lax.all_gather(normed, "tp", axis=0, tiled=True)
    gate = jnp.dot(
        span_rows,
        lax.all_gather(gate_weight, "sp", axis=0, tiled=True),
        preferred_element_type=jnp.float32,
    )
    upper = jnp.dot(
        span_rows,
        lax.all_gather(up_weight, "sp", axis=0, tiled=True),
        preferred_element_type=jnp.float32,
    )
    hidden = (jax.nn.silu(gate) * upper).astype(jnp.bfloat16)
    partial_out = jnp.dot(
        hidden,
        lax.all_gather(down_weight, "sp", axis=1, tiled=True),
        preferred_element_type=jnp.float32,
    )
    feed = lax.psum_scatter(
        partial_out.astype(jnp.bfloat16), "tp", scatter_dimension=0, tiled=True
    ).astype(jnp.float32)
    return (stream + feed).astype(jnp.bfloat16)


def solution(mesh):
    in_specs = (
        P(("sp", "tp"), None),
        P("sp", "tp"),
        P("sp", "tp"),
        P("sp", "tp"),
        P("sp"),
        P("tp"),
        P("tp", None),
        P(),
        P("sp", "tp"),
        P("sp", "tp"),
        P("tp", "sp"),
    )
    out_specs = P(("sp", "tp"), None)
    return jax.shard_map(
        on_device, mesh=mesh, in_specs=in_specs, out_specs=out_specs, check_vma=False
    )
```

profile of v0, /device:TPU:0, one launch (start us, length us, event | category | flops | bytes accessed | tf_op | source)
XLA Modules:
  0.0 761.2 jit_solution(9639619573280566356)
XLA Ops:
  8.5 4.9 collective-permute-start.4
  14.5 3.4 collective-permute-start.3
  17.9 2.1 collective-permute-done.4
  20.1 5.3 collective-permute-start.6
  25.6 4.6 collective-permute-start.5
  30.2 7.5 collective-permute-done.6
  38.9 7.6 %collective-permute-start.8 = (bf16[512,1024]{0,1:T(8,128)(2,1)}, bf16[512,1024]{0,1:T(8,128)(2,1)}, u32[]{:S(2)}, u32[]{:S(2)}) collective-permute-start(bf16[512,1024]{0,1:T(8,128)(2,1)} %pad_maximum_fusion.1), channel_id=1, source_target_pairs={{0,8},{2,10},{4,12},{6,14},{8,16},{10,18},{12,20},{14,22},{16,24},... | collective-permute-start | bytes 3145736 | tf_op jit(solution)/shard_map/ppermute | solution.py:10
  49.1 8.6 %collective-permute-start.7 = (bf16[512,1024]{0,1:T(8,128)(2,1)}, bf16[512,1024]{0,1:T(8,128)(2,1)}, u32[]{:S(2)}, u32[]{:S(2)}) collective-permute-start(bf16[512,1024]{0,1:T(8,128)(2,1)} %pad_maximum_fusion), channel_id=1, source_target_pairs={{0,8},{2,10},{4,12},{6,14},{8,16},{10,18},{12,20},{14,22},{16,24},... | collective-permute-start | bytes 3145736 | tf_op jit(solution)/shard_map/ppermute | solution.py:10
  60.3 5.3 collective-permute-start.1
  67.0 37.6 %collective-permute-start.2 = (s32[512]{0:T(512)S(1)}, s32[512]{0:T(512)S(1)}, u32[]{:S(2)}, u32[]{:S(2)}) collective-permute-start(s32[512]{0:T(512)S(1)} %pad_add_fusion), channel_id=1, source_target_pairs={{0,8},{2,10},{4,12},{6,14},{8,16},{10,18},{12,20},{14,22},{16,24},... | collective-permute-start | bytes 6152 | tf_op jit(solution)/shard_map/ppermute | solution.py:10
  111.1 17.5 %conditional.4 = (f32[128,16,64]{0,2,1:T(8,128)S(1)}, f32[16,128]{1,0:T(8,128)S(1)}) conditional(s32[]{:T(128)} %convert_element_type.66, () %tuple.49, (s32[]{:T(128)}, s32[128]{0:T(128)S(1)}, s32[256]{0:T(256)S(1)}, s32[128]{0:T(128)S(1)}, bf16[256,1024]{0,1:T(8,128)(2,1)S(1)}, /*index=5*/bf16[128,16,64]{0,2,1:T(8,128)(2,1)S(1)}, f32[16]{0:T(128)S(1)}, ...), branch_computations={%region_0.0_spmd, %region_1.5_spmd} | conditional | flops 223449856 | bytes 37884532 | solution.py:56
  115.4 5.9 fusion.53
  123.3 5.2 convolution_bitcast_fusion.1
  129.0 7.0 conditional.6
  136.0 8.4 %conditional.7 = (f32[128,16,64]{0,2,1:T(8,128)S(1)}) conditional(s32[]{:T(128)} %convert_element_type.63, f32[128,16,64]{0,2,1:T(8,128)S(1)} %get-tuple-element.181, (s32[]{:T(128)}, s32[128]{0:T(128)S(1)}, s32[512]{0:T(512)S(1)}, s32[128]{0:T(128)S(1)}, bf16[512,1024]{0,1:T(8,128)(2,1)}, /*index=5*/bf16[128,16,64]{0,2,1:T(8,128)(2,1)S(1)}, ...), branch_computations={%region_15.16_spmd, %region_16.19_spmd} | conditional | flops 218897152 | bytes 29825692 | solution.py:56
  144.5 3.7 convolution_convert_fusion.1
  150.0 88.4 %reduce-scatter.3.cloned.1.call-done = bf16[64,2048]{1,0:T(8,128)(2,1)} async-done(((bf16[128,2048]{1,0:T(8,128)(2,1)}), bf16[64,2048]{1,0:T(8,128)(2,1)}) %reduce-scatter.3.cloned.1.call-update) | async-done | bytes 262160 | tf_op jit(solution)/shard_map/reduce_scatter | solution.py:100
  240.7 2.2 all_gather.12
  242.9 141.8 %all-gather.4.cloned.1.call-done = bf16[2048,3072]{1,0:T(8,128)(2,1)} async-done(((bf16[128,3072]{1,0:T(8,128)(2,1)}), bf16[2048,3072]{1,0:T(8,128)(2,1)}) %all-gather.4.cloned.1.call-update) | async-done | bytes 12582928 | tf_op jit(solution)/shard_map/all_gather | solution.py:113
  384.7 6.4 fusion.56
  391.1 145.5 %all-gather.6.cloned.1.call-done = bf16[2048,3072]{1,0:T(8,128)(2,1)} async-done(((bf16[128,3072]{1,0:T(8,128)(2,1)}), bf16[2048,3072]{1,0:T(8,128)(2,1)}) %all-gather.6.cloned.1.call-update) | async-done | bytes 12582928 | tf_op jit(solution)/shard_map/all_gather | solution.py:118
  536.6 196.1 %all-gather.8.cloned.1.call-done = bf16[3072,2048]{1,0:T(8,128)(2,1)} async-done(((bf16[3072,128]{1,0:T(8,128)(2,1)}), bf16[3072,2048]{1,0:T(8,128)(2,1)}) %all-gather.8.cloned.1.call-update) | async-done | bytes 12582928 | tf_op jit(solution)/shard_map/all_gather | solution.py:124
  732.7 12.7 %convolution_convert_fusion = bf16[128,2048]{1,0:T(8,128)(2,1)} fusion(bf16[3072,2048]{1,0:T(8,128)(2,1)} %all-gather.8.cloned.1.call-done, bf16[128,2048]{1,0:T(8,128)(2,1)S(1)} %all_gather.12, bf16[2048,3072]{1,0:T(8,128)(2,1)} %all-gather.6.cloned.1.call-done, f32[128,3072]{1,0:T(8,128)S(1)} %fusion.56), kind=kOutput, calls=%fused_computation.87 | convolution fusion | flops 3223846912 | bytes 27787264 | tf_op jit(solution)/shard_map/dot_general | solution.py:122
  745.4 6.3 reduce-scatter.5.cloned.1.call-done
  (67 shorter events, 23.9 us)
Async XLA Ops:
  7.4 231.1 %reduce-scatter.3.cloned.1.call-start = ((), (), s32[]{:S(2)}) async-start(), calls=%async_computation.2 | async-start | bytes 786432 | tf_op jit(solution)/shard_map/reduce_scatter | solution.py:100
  8.5 11.6 %collective-permute-start.4 = (bf16[128,1024]{0,1:T(8,128)(2,1)S(1)}, bf16[128,1024]{0,1:T(8,128)(2,1)S(1)}, u32[]{:S(2)}, u32[]{:S(2)}) collective-permute-start(bf16[128,1024]{0,1:T(8,128)(2,1)S(1)} %copy.23), channel_id=1, source_target_pairs={{0,2},{2,4},{4,6},{6,8},{8,10},{10,12},{12,14},{14,16},{16,18},{18... | collective-permute-start | bytes 786440 | tf_op jit(solution)/shard_map/ppermute | solution.py:10
  14.5 11.0 %collective-permute-start.3 = (bf16[128,1024]{0,1:T(8,128)(2,1)S(1)}, bf16[128,1024]{0,1:T(8,128)(2,1)S(1)}, u32[]{:S(2)}, u32[]{:S(2)}) collective-permute-start(bf16[128,1024]{0,1:T(8,128)(2,1)S(1)} %copy.20), channel_id=1, source_target_pairs={{0,2},{2,4},{4,6},{6,8},{8,10},{10,12},{12,14},{14,16},{16,18},{18... | collective-permute-start | bytes 786440 | tf_op jit(solution)/shard_map/ppermute | solution.py:10
  20.1 17.6 %collective-permute-start.6 = (bf16[256,1024]{0,1:T(8,128)(2,1)S(1)}, bf16[256,1024]{0,1:T(8,128)(2,1)S(1)}, u32[]{:S(2)}, u32[]{:S(2)}) collective-permute-start(bf16[256,1024]{0,1:T(8,128)(2,1)S(1)} %pad_maximum_fusion.3), channel_id=1, source_target_pairs={{0,4},{2,6},{4,8},{6,10},{8,12},{10,14},{12,16},{14,18},{16,20},{1... | collective-permute-start | bytes 1572872 | tf_op jit(solution)/shard_map/ppermute | solution.py:10
  25.5 32.2 %copy-start.9 = (s32[128]{0:T(128)S(1)}, s32[128]{0:T(128)}, u32[]{:S(2)}) copy-start(s32[128]{0:T(128)} %param.23) | copy-start | bytes 1540
  25.6 79.1 %copy-start.8 = (bf16[128,1024]{1,0:T(8,128)(2,1)S(1)}, bf16[128,1024]{1,0:T(8,128)(2,1)}, u32[]{:S(2)}) copy-start(bf16[128,1024]{1,0:T(8,128)(2,1)} %param.20) | copy-start | bytes 786436
  25.6 85.5 %copy-start.11 = (f32[16]{0:T(128)S(1)}, f32[16]{0:T(128)}, u32[]{:S(2)}) copy-start(f32[16]{0:T(128)} %param.24) | copy-start | bytes 196
  25.6 22.4 %collective-permute-start.5 = (bf16[256,1024]{0,1:T(8,128)(2,1)S(1)}, bf16[256,1024]{0,1:T(8,128)(2,1)S(1)}, u32[]{:S(2)}, u32[]{:S(2)}) collective-permute-start(bf16[256,1024]{0,1:T(8,128)(2,1)S(1)} %pad_maximum_fusion.2), channel_id=1, source_target_pairs={{0,4},{2,6},{4,8},{6,10},{8,12},{10,14},{12,16},{14,18},{16,20},{1... | collective-permute-start | bytes 1572872 | tf_op jit(solution)/shard_map/ppermute | solution.py:10
  37.7 11.4 %copy-start.5 = (bf16[256,1024]{0,1:T(8,128)(2,1)}, bf16[256,1024]{0,1:T(8,128)(2,1)S(1)}, u32[]{:S(2)}) copy-start(bf16[256,1024]{0,1:T(8,128)(2,1)S(1)} %collective-permute-done.6) | copy-start | bytes 1572868
  38.9 90.1 %collective-permute-start.8 = (bf16[512,1024]{0,1:T(8,128)(2,1)}, bf16[512,1024]{0,1:T(8,128)(2,1)}, u32[]{:S(2)}, u32[]{:S(2)}) collective-permute-start(bf16[512,1024]{0,1:T(8,128)(2,1)} %pad_maximum_fusion.1), channel_id=1, source_target_pairs={{0,8},{2,10},{4,12},{6,14},{8,16},{10,18},{12,20},{14,22},{16,24},... | collective-permute-start | bytes 3145736 | tf_op jit(solution)/shard_map/ppermute | solution.py:10
  47.9 63.1 %copy-start.7 = (bf16[256,1024]{0,1:T(8,128)(2,1)}, bf16[256,1024]{0,1:T(8,128)(2,1)S(1)}, u32[]{:S(2)}) copy-start(bf16[256,1024]{0,1:T(8,128)(2,1)S(1)} %collective-permute-done.5) | copy-start | bytes 1572868
  49.1 79.9 %collective-permute-start.7 = (bf16[512,1024]{0,1:T(8,128)(2,1)}, bf16[512,1024]{0,1:T(8,128)(2,1)}, u32[]{:S(2)}, u32[]{:S(2)}) collective-permute-start(bf16[512,1024]{0,1:T(8,128)(2,1)} %pad_maximum_fusion), channel_id=1, source_target_pairs={{0,8},{2,10},{4,12},{6,14},{8,16},{10,18},{12,20},{14,22},{16,24},... | collective-permute-start | bytes 3145736 | tf_op jit(solution)/shard_map/ppermute | solution.py:10
  57.7 2.6 collective-permute-start
  60.3 6.6 collective-permute-start.1
  67.0 41.0 %collective-permute-start.2 = (s32[512]{0:T(512)S(1)}, s32[512]{0:T(512)S(1)}, u32[]{:S(2)}, u32[]{:S(2)}) collective-permute-start(s32[512]{0:T(512)S(1)} %pad_add_fusion), channel_id=1, source_target_pairs={{0,8},{2,10},{4,12},{6,14},{8,16},{10,18},{12,20},{14,22},{16,24},... | collective-permute-start | bytes 6152 | tf_op jit(solution)/shard_map/ppermute | solution.py:10
  111.9 1.5 copy-start.4
  148.2 90.3 %copy-start = (bf16[64,2048]{1,0:T(8,128)(2,1)S(1)}, bf16[64,2048]{1,0:T(8,128)(2,1)}, u32[]{:S(2)}) copy-start(bf16[64,2048]{1,0:T(8,128)(2,1)} %param.19) | copy-start | bytes 786436
  148.2 91.4 %copy-start.10 = (f32[2048]{0:T(1024)S(1)}, f32[2048]{0:T(1024)}, u32[]{:S(2)}) copy-start(f32[2048]{0:T(1024)} %param.26) | copy-start | bytes 24580
  148.2 236.5 %all-gather.4.cloned.1.call-start = ((), (), s32[]{:S(2)}) async-start(), calls=%async_computation.3 | async-start | bytes 13369344 | tf_op jit(solution)/shard_map/all_gather | solution.py:113
  148.8 387.8 %all-gather.6.cloned.1.call-start = ((), (), s32[]{:S(2)}) async-start(), calls=%async_computation.4 | async-start | bytes 13369344 | tf_op jit(solution)/shard_map/all_gather | solution.py:118
  149.4 583.3 %all-gather.8.cloned.1.call-start = ((), (), s32[]{:S(2)}) async-start(), calls=%async_computation.5 | async-start | bytes 13369344 | tf_op jit(solution)/shard_map/all_gather | solution.py:124
  150.0 601.7 %reduce-scatter.5.cloned.1.call-start = ((), (), s32[]{:S(2)}) async-start(), calls=%async_computation.6 | async-start | bytes 786432 | tf_op jit(solution)/shard_map/reduce_scatter | solution.py:127
  391.1 360.6 %copy-start.1 = (bf16[64,2048]{1,0:T(8,128)(2,1)S(1)}, bf16[64,2048]{1,0:T(8,128)(2,1)}, u32[]{:S(2)}) copy-start(bf16[64,2048]{1,0:T(8,128)(2,1)} %reduce-scatter.3.cloned.1.call-done) | copy-start | bytes 786436
Sparse Core Ops, SparseCore 0:
  148.4 90.0 reduce-scatter.2
  745.5 6.0 reduce-scatter.4
Sparse Core Ops, SparseCore 1:
  151.5 233.2 all-gather.3
  387.4 149.2 all-gather.5
  539.2 193.4 all-gather.7
where the time goes:
time: 771 us; the launch traced here: 761 us
  waiting for transfers between devices  593 us (77%)
  starting transfers between devices  79 us (10%)
  matrix products  28.7 us (4%)
  between operations  20.5 us (3%)
  loops' own time  16 us (2%)
  other arithmetic  14.1 us (2%)
  local copies, waits for them, and re-layouts  8.17 us (1%)
    all_gather x1, waiting for transfers between devices, on_device(): lax.all_gather(down_weight, 'sp', axis=1, tiled=True)  196 us
    all_gather x1, waiting for transfers between devices, on_device(): lax.all_gather(up_weight, 'sp', axis=0, tiled=True)  146 us
    all_gather x1, waiting for transfers between devices, on_device(): lax.all_gather(gate_weight, 'sp', axis=0, tiled=True)  142 us
    reduce_scatter x1, waiting for transfers between devices, on_device(): lax.psum_scatter(jnp.dot(attended, out_weight, preferred_element_type=jnp...  88.4 us
    ppermute x9, starting transfers between devices, from_behind(): return lax.ppermute(shard, axis, pairs)  78.8 us
    another operation x4, loops' own time, block_update(): return lax.cond(reached, compute, lambda: carry)  16 us
  transfers between devices with their start and end apart: 14, of which 10 were waited for; matrix products, arithmetic and copies ran while one was open for 4% of the time, Pallas kernels for 0%

commit v1 on v0

--- a/solution.py
+++ b/solution.py
@@ -2,6 +2,11 @@
 import jax.numpy as jnp
 from jax import lax
 from jax.sharding import PartitionSpec as P
+
+
+def swapped_in(x, name, along):
+    stack = jnp.stack([x] * lax.axis_size(name))
+    return jnp.concatenate(lax.all_to_all(stack, name, 0, 0), axis=along)
 
 
 def from_behind(shard, axis, by):
@@ -113,11 +118,7 @@
         lax.all_gather(gate_weight, "sp", axis=0, tiled=True),
         preferred_element_type=jnp.float32,
     )
-    upper = jnp.dot(
-        span_rows,
-        lax.all_gather(up_weight, "sp", axis=0, tiled=True),
-        preferred_element_type=jnp.float32,
-    )
+    upper = jnp.dot(span_rows, swapped_in(up_weight, "sp", 0), preferred_element_type=jnp.float32)
     hidden = (jax.nn.silu(gate) * upper).astype(jnp.bfloat16)
     partial_out = jnp.dot(
         hidden,

time: 771 us -> 859 us (1.11)
  starting transfers between devices: 79 us -> 170 us
    all_gather x1, waiting for transfers between devices: 142 us -> 367 us  [on_device(): lax.all_gather(gate_weight, 'sp', axis=0, tiled=True)]
    all_gather x1 -> x0, waiting for transfers between devices: 146 us -> none  [on_device(): lax.all_gather(up_weight, 'sp', axis=0, tiled=True)]
    all_to_all x0 -> x1, starting transfers between devices: none -> 90.9 us  [swapped_in(): return jnp.concatenate(lax.all_to_all(stack, name, 0, 0), axis=along)]
    reduce_scatter x1, waiting for transfers between devices: 88.4 us -> 0.02 us  [on_device(): lax.psum_scatter(jnp.dot(attended, out_weight, preferred_element_type=jnp...]
  transfers between devices with their start and end apart: 14 -> 14, of which waited for: 10 -> 8; matrix products, arithmetic and copies ran while one was open for 4% -> 4% of each run, Pallas kernels for 0% -> 0%
where the time goes in v1:
time: 859 us; the launch traced here: 849 us
  waiting for transfers between devices  587 us (68%)
  starting transfers between devices  170 us (20%)
  matrix products  28.8 us (3%)
  between operations  20.4 us (2%)
  local copies, waits for them, and re-layouts  14.3 us (2%)
  other arithmetic  14.1 us (2%)
  loops' own time  13.1 us (2%)
    all_gather x1, waiting for transfers between devices, on_device(): lax.all_gather(gate_weight, 'sp', axis=0, tiled=True)  367 us
    all_gather x1, waiting for transfers between devices, on_device(): lax.all_gather(down_weight, 'sp', axis=1, tiled=True)  199 us
    all_to_all x1, starting transfers between devices, swapped_in(): return jnp.concatenate(lax.all_to_all(stack, name, 0, 0), axis=along)  90.9 us
    ppermute x9, starting transfers between devices, from_behind(): return lax.ppermute(shard, axis, pairs)  78.8 us
  transfers between devices with their start and end apart: 14, of which 8 were waited for; matrix products, arithmetic and copies ran while one was open for 4% of the time, Pallas kernels for 0%

profile of v1, /device:TPU:0, one launch (start us, length us, event | category | flops | bytes accessed | tf_op | source)
XLA Modules:
  0.0 849.5 jit_solution(5705848690438821208)
XLA Ops:
  8.5 4.9 collective-permute-start.4
  14.5 3.4 collective-permute-start.3
  17.9 2.1 collective-permute-done.4
  20.1 5.3 collective-permute-start.6
  25.6 4.6 collective-permute-start.5
  30.2 7.5 collective-permute-done.6
  38.9 7.6 collective-permute-start.8
  49.1 8.6 %collective-permute-start.7 = (bf16[512,1024]{0,1:T(8,128)(2,1)}, bf16[512,1024]{0,1:T(8,128)(2,1)}, u32[]{:S(2)}, u32[]{:S(2)}) collective-permute-start(bf16[512,1024]{0,1:T(8,128)(2,1)} %pad_maximum_fusion), channel_id=1, source_target_pairs={{0,8},{2,10},{4,12},{6,14},{8,16},{10,18},{12,20},{14,22},{16,24},... | collective-permute-start | bytes 3145736 | tf_op jit(solution)/shard_map/ppermute | solution.py:15
  60.3 5.3 collective-permute-start.1
  67.0 37.7 %collective-permute-start.2 = (s32[512]{0:T(512)S(1)}, s32[512]{0:T(512)S(1)}, u32[]{:S(2)}, u32[]{:S(2)}) collective-permute-start(s32[512]{0:T(512)S(1)} %pad_add_fusion), channel_id=1, source_target_pairs={{0,8},{2,10},{4,12},{6,14},{8,16},{10,18},{12,20},{14,22},{16,24},... | collective-permute-start | bytes 6152 | tf_op jit(solution)/shard_map/ppermute | solution.py:15
  111.1 17.4 %conditional.4 = (f32[128,16,64]{0,2,1:T(8,128)S(1)}, f32[16,128]{1,0:T(8,128)S(1)}) conditional(s32[]{:T(128)} %convert_element_type.66, () %tuple.49, (s32[]{:T(128)}, s32[128]{0:T(128)S(1)}, s32[256]{0:T(256)S(1)}, s32[128]{0:T(128)S(1)}, bf16[256,1024]{0,1:T(8,128)(2,1)S(1)}, /*index=5*/bf16[128,16,64]{0,2,1:T(8,128)(2,1)S(1)}, f32[16]{0:T(128)S(1)}, ...), branch_computations={%region_0.0_spmd, %region_1.5_spmd} | conditional | flops 223449856 | bytes 37884532 | solution.py:61
  115.4 5.9 fusion.53
  123.3 5.2 convolution_bitcast_fusion.1
  129.1 7.0 conditional.6
  136.0 5.5 conditional.7
  141.6 3.8 convolution_convert_fusion.1
  146.0 6.1 stack.2
  152.1 90.9 %all-to-all-start = ((bf16[16,128,3072]{2,1,0:T(8,128)(2,1)}), bf16[16,128,3072]{2,1,0:T(8,128)(2,1)}, u32[]{:S(2)}, u32[]{:S(2)}) async-start(bf16[16,128,3072]{2,1,0:T(8,128)(2,1)} %stack.2), calls=%async_computation.1 | async-start | bytes 25165824 | tf_op jit(solution)/shard_map/all_to_all | solution.py:9
  245.9 2.4 all_gather.9
  248.4 367.4 %all-gather.3.cloned.1.call-done = bf16[2048,3072]{1,0:T(8,128)(2,1)} async-done(((bf16[128,3072]{1,0:T(8,128)(2,1)}), bf16[2048,3072]{1,0:T(8,128)(2,1)}) %all-gather.3.cloned.1.call-update) | async-done | bytes 12582928 | tf_op jit(solution)/shard_map/all_gather | solution.py:118
  615.8 6.4 fusion.56
  622.2 198.8 %all-gather.5.cloned.1.call-done = bf16[3072,2048]{1,0:T(8,128)(2,1)} async-done(((bf16[3072,128]{1,0:T(8,128)(2,1)}), bf16[3072,2048]{1,0:T(8,128)(2,1)}) %all-gather.5.cloned.1.call-update) | async-done | bytes 12582928 | tf_op jit(solution)/shard_map/all_gather | solution.py:125
  821.0 12.7 %convolution_convert_fusion = bf16[128,2048]{1,0:T(8,128)(2,1)} fusion(bf16[3072,2048]{1,0:T(8,128)(2,1)} %all-gather.5.cloned.1.call-done, bf16[128,2048]{1,0:T(8,128)(2,1)S(1)} %all_gather.9, bf16[2048,3072]{1,0:T(8,128)(2,1)} %bitcast.24, f32[128,3072]{1,0:T(8,128)S(1)} %fusion.56), kind=kOutput, calls=%fused_computation.87 | convolution fusion | flops 3223846912 | bytes 27787264 | tf_op jit(solution)/shard_map/dot_general | solution.py:123
  833.8 6.3 reduce-scatter.5.cloned.1.call-done
  (69 shorter events, 23.4 us)
Async XLA Ops:
  7.4 236.3 %reduce-scatter.3.cloned.1.call-start = ((), (), s32[]{:S(2)}) async-start(), calls=%async_computation.3 | async-start | bytes 786432 | tf_op jit(solution)/shard_map/reduce_scatter | solution.py:105
  8.5 11.6 %collective-permute-start.4 = (bf16[128,1024]{0,1:T(8,128)(2,1)S(1)}, bf16[128,1024]{0,1:T(8,128)(2,1)S(1)}, u32[]{:S(2)}, u32[]{:S(2)}) collective-permute-start(bf16[128,1024]{0,1:T(8,128)(2,1)S(1)} %copy.23), channel_id=1, source_target_pairs={{0,2},{2,4},{4,6},{6,8},{8,10},{10,12},{12,14},{14,16},{16,18},{18... | collective-permute-start | bytes 786440 | tf_op jit(solution)/shard_map/ppermute | solution.py:15
  14.5 11.0 %collective-permute-start.3 = (bf16[128,1024]{0,1:T(8,128)(2,1)S(1)}, bf16[128,1024]{0,1:T(8,128)(2,1)S(1)}, u32[]{:S(2)}, u32[]{:S(2)}) collective-permute-start(bf16[128,1024]{0,1:T(8,128)(2,1)S(1)} %copy.20), channel_id=1, source_target_pairs={{0,2},{2,4},{4,6},{6,8},{8,10},{10,12},{12,14},{14,16},{16,18},{18... | collective-permute-start | bytes 786440 | tf_op jit(solution)/shard_map/ppermute | solution.py:15
  20.1 17.6 %collective-permute-start.6 = (bf16[256,1024]{0,1:T(8,128)(2,1)S(1)}, bf16[256,1024]{0,1:T(8,128)(2,1)S(1)}, u32[]{:S(2)}, u32[]{:S(2)}) collective-permute-start(bf16[256,1024]{0,1:T(8,128)(2,1)S(1)} %pad_maximum_fusion.3), channel_id=1, source_target_pairs={{0,4},{2,6},{4,8},{6,10},{8,12},{10,14},{12,16},{14,18},{16,20},{1... | collective-permute-start | bytes 1572872 | tf_op jit(solution)/shard_map/ppermute | solution.py:15
  25.5 32.2 %copy-start.10 = (s32[128]{0:T(128)S(1)}, s32[128]{0:T(128)}, u32[]{:S(2)}) copy-start(s32[128]{0:T(128)} %param.23) | copy-start | bytes 1540
  25.6 79.1 %copy-start.9 = (bf16[128,1024]{1,0:T(8,128)(2,1)S(1)}, bf16[128,1024]{1,0:T(8,128)(2,1)}, u32[]{:S(2)}) copy-start(bf16[128,1024]{1,0:T(8,128)(2,1)} %param.20) | copy-start | bytes 786436
  25.6 85.5 %copy-start.12 = (f32[16]{0:T(128)S(1)}, f32[16]{0:T(128)}, u32[]{:S(2)}) copy-start(f32[16]{0:T(128)} %param.24) | copy-start | bytes 196
  25.6 22.4 %collective-permute-start.5 = (bf16[256,1024]{0,1:T(8,128)(2,1)S(1)}, bf16[256,1024]{0,1:T(8,128)(2,1)S(1)}, u32[]{:S(2)}, u32[]{:S(2)}) collective-permute-start(bf16[256,1024]{0,1:T(8,128)(2,1)S(1)} %pad_maximum_fusion.2), channel_id=1, source_target_pairs={{0,4},{2,6},{4,8},{6,10},{8,12},{10,14},{12,16},{14,18},{16,20},{1... | collective-permute-start | bytes 1572872 | tf_op jit(solution)/shard_map/ppermute | solution.py:15
  37.7 21.3 %copy-start.6 = (bf16[256,1024]{0,1:T(8,128)(2,1)}, bf16[256,1024]{0,1:T(8,128)(2,1)S(1)}, u32[]{:S(2)}) copy-start(bf16[256,1024]{0,1:T(8,128)(2,1)S(1)} %collective-permute-done.6) | copy-start | bytes 1572868
  38.9 90.2 %collective-permute-start.8 = (bf16[512,1024]{0,1:T(8,128)(2,1)}, bf16[512,1024]{0,1:T(8,128)(2,1)}, u32[]{:S(2)}, u32[]{:S(2)}) collective-permute-start(bf16[512,1024]{0,1:T(8,128)(2,1)} %pad_maximum_fusion.1), channel_id=1, source_target_pairs={{0,8},{2,10},{4,12},{6,14},{8,16},{10,18},{12,20},{14,22},{16,24},... | collective-permute-start | bytes 3145736 | tf_op jit(solution)/shard_map/ppermute | solution.py:15
  47.9 63.1 %copy-start.8 = (bf16[256,1024]{0,1:T(8,128)(2,1)}, bf16[256,1024]{0,1:T(8,128)(2,1)S(1)}, u32[]{:S(2)}) copy-start(bf16[256,1024]{0,1:T(8,128)(2,1)S(1)} %collective-permute-done.5) | copy-start | bytes 1572868
  49.1 80.0 %collective-permute-start.7 = (bf16[512,1024]{0,1:T(8,128)(2,1)}, bf16[512,1024]{0,1:T(8,128)(2,1)}, u32[]{:S(2)}, u32[]{:S(2)}) collective-permute-start(bf16[512,1024]{0,1:T(8,128)(2,1)} %pad_maximum_fusion), channel_id=1, source_target_pairs={{0,8},{2,10},{4,12},{6,14},{8,16},{10,18},{12,20},{14,22},{16,24},... | collective-permute-start | bytes 3145736 | tf_op jit(solution)/shard_map/ppermute | solution.py:15
  57.7 2.6 collective-permute-start
  60.3 6.6 collective-permute-start.1
  67.0 41.0 %collective-permute-start.2 = (s32[512]{0:T(512)S(1)}, s32[512]{0:T(512)S(1)}, u32[]{:S(2)}, u32[]{:S(2)}) collective-permute-start(s32[512]{0:T(512)S(1)} %pad_add_fusion), channel_id=1, source_target_pairs={{0,8},{2,10},{4,12},{6,14},{8,16},{10,18},{12,20},{14,22},{16,24},... | collective-permute-start | bytes 6152 | tf_op jit(solution)/shard_map/ppermute | solution.py:15
  111.9 1.5 copy-start.4
  141.6 4.4 copy-start.5
  145.4 470.4 %all-gather.3.cloned.1.call-start = ((), (), s32[]{:S(2)}) async-start(), calls=%async_computation.4 | async-start | bytes 13369344 | tf_op jit(solution)/shard_map/all_gather | solution.py:118
  152.1 91.6 %copy-start = (bf16[64,2048]{1,0:T(8,128)(2,1)S(1)}, bf16[64,2048]{1,0:T(8,128)(2,1)}, u32[]{:S(2)}) copy-start(bf16[64,2048]{1,0:T(8,128)(2,1)} %param.19) | copy-start | bytes 786436
  152.1 92.7 %copy-start.11 = (f32[2048]{0:T(1024)S(1)}, f32[2048]{0:T(1024)}, u32[]{:S(2)}) copy-start(f32[2048]{0:T(1024)} %param.26) | copy-start | bytes 24580
  152.1 470.1 %all-to-all-start = ((bf16[16,128,3072]{2,1,0:T(8,128)(2,1)}), bf16[16,128,3072]{2,1,0:T(8,128)(2,1)}, u32[]{:S(2)}, u32[]{:S(2)}) async-start(bf16[16,128,3072]{2,1,0:T(8,128)(2,1)} %stack.2), calls=%async_computation.1 | async-start | bytes 25165824 | tf_op jit(solution)/shard_map/all_to_all | solution.py:9
  243.0 578.0 %all-gather.5.cloned.1.call-start = ((), (), s32[]{:S(2)}) async-start(), calls=%async_computation.5 | async-start | bytes 13369344 | tf_op jit(solution)/shard_map/all_gather | solution.py:125
  243.6 596.4 %reduce-scatter.5.cloned.1.call-start = ((), (), s32[]{:S(2)}) async-start(), calls=%async_computation.6 | async-start | bytes 786432 | tf_op jit(solution)/shard_map/reduce_scatter | solution.py:128
  821.0 19.0 %copy-start.1 = (bf16[64,2048]{1,0:T(8,128)(2,1)S(1)}, bf16[64,2048]{1,0:T(8,128)(2,1)}, u32[]{:S(2)}) copy-start(bf16[64,2048]{1,0:T(8,128)(2,1)} %reduce-scatter.3.cloned.1.call-done) | copy-start | bytes 786436
Sparse Core Ops, SparseCore 0:
  145.5 93.0 reduce-scatter.2
  833.9 6.0 reduce-scatter.4
Sparse Core Ops, SparseCore 1:
  148.7 467.1 all-gather.2
  618.4 202.6 all-gather.4
